TPU v7x, 32 devices: a whole 2x2x4 slice. The times are simulated.
32 devices in a mesh: rep: 2 (over x), fs: 8 (over z, y), tp: 2 (over core).
Axes of the slice: x: 2, y: 2, z: 4, core: 2. Of those that a mesh axis runs over, the one named last changes fastest.
Arguments:
- tokens: bfloat16 [16384, 2048], P(('rep', 'fs')), may hold values from -6 to 6
- norm_mix: bfloat16 [2048], replicated, may hold values from 0.099609375 to 1.8984375
- w_unit: bfloat16 [2048, 1024], P('fs', 'tp'), may hold values from -0.125 to 0.125
- w_value: bfloat16 [2048, 1024], P('fs', 'tp'), may hold values from -0.125 to 0.125
- spatial: bfloat16 [4, 128, 128], replicated, may hold values from -0.52734375 to 0.52734375
- spatial_bias: bfloat16 [4, 128], replicated, may hold values from 0.099609375 to 1.8984375
- group_gain: bfloat16 [1024], replicated, may hold values from 0.099609375 to 1.8984375
- group_shift: bfloat16 [1024], replicated, may hold values from -3 to 3
- w_mix_out: bfloat16 [1024, 2048], P('tp', 'fs'), may hold values from -0.1875 to 0.1875
- norm_ffn: bfloat16 [2048], replicated, may hold values from 0.099609375 to 1.8984375
- w_gate: bfloat16 [2048, 2816], P('fs', 'tp'), may hold values from -0.125 to 0.125
- w_up: bfloat16 [2048, 2816], P('fs', 'tp'), may hold values from -0.125 to 0.125
- w_down: bfloat16 [2816, 2048], P('tp', 'fs'), may hold values from -0.109375 to 0.109375
Outputs:
- layer_out: bfloat16 [16384, 2048], P(('rep', 'fs', 'tp'))
All inputs are finite; a program needn't handle non-finite values.
Results may differ from a plain program's by a relative error of at most 0.008.
Values may be sent and summed in bfloat16 or wider, within the bound.
A program may use at most 128 MiB of HBM per device.

v0:
```python
import jax
import jax.numpy as jnp
from jax import lax
from jax.sharding import PartitionSpec as P


def rms_scale(values, gain):
    values = values.astype(jnp.float32)
    scale = lax.rsqrt(jnp.mean(values * values, axis=-1, keepdims=True) + 1e-06)
    return values * scale * gain.astype(jnp.float32)


def spatial_unit(unit_pre, value_pre, spatial, spatial_bias, group_gain, group_shift):
    count, width = value_pre.shape
    groups = spatial.shape[0]
    block = spatial.shape[1]
    active = jax.nn.gelu(value_pre, approximate=True).reshape(count, groups, width // groups)
    center = jnp.mean(active, axis=-1, keepdims=True)
    spread = jnp.mean(jnp.square(active - center), axis=-1, keepdims=True)
    normal = ((active - center) * lax.rsqrt(spread + 1e-06)).reshape(count, width)
    normal = normal * group_gain.astype(jnp.float32) + group_shift.astype(jnp.float32)
    grouped = normal.astype(jnp.bfloat16)
    causal = jnp.tril(jnp.ones((block, block), dtype=bool))
    weights = jnp.where(causal[None], spatial, jnp.zeros_like(spatial))
    tiles = grouped.reshape(count // block, block, groups, width // groups)
    mixed = jnp.einsum("gts,nsgd->ntgd", weights, tiles, preferred_element_type=jnp.float32)
    mixed = mixed + spatial_bias.astype(jnp.float32).T[None, :, :, None]
    return jax.nn.gelu(unit_pre, approximate=True) * mixed.reshape(count, width)


def on_device(
    tokens,
    norm_mix,
    w_unit,
    w_value,
    spatial,
    spatial_bias,
    group_gain,
    group_shift,
    w_mix_out,
    norm_ffn,
    w_gate,
    w_up,
    w_down,
):
    count = tokens.shape[0]
    half = count // lax.axis_size("tp")
    position = lax.axis_index("tp")
    row_start = position * half
    local_width = w_unit.shape[1]
    group_count = spatial.shape[0] // lax.axis_size("tp")
    group_start = position * group_count
    spatial_local = lax.dynamic_slice_in_dim(spatial, group_start, group_count, 0)
    bias_local = lax.dynamic_slice_in_dim(spatial_bias, group_start, group_count, 0)
    gain_local = lax.dynamic_slice_in_dim(group_gain, position * local_width, local_width, 0)
    shift_local = lax.dynamic_slice_in_dim(group_shift, position * local_width, local_width, 0)
    normed = rms_scale(tokens, norm_mix).astype(jnp.bfloat16)
    unit_whole, value_whole = (
        lax.all_gather(w_unit, "fs", axis=0, tiled=True),
        lax.all_gather(w_value, "fs", axis=0, tiled=True),
    )
    unit_pre = jnp.dot(normed, unit_whole, preferred_element_type=jnp.float32)
    value_pre = jnp.dot(normed, value_whole, preferred_element_type=jnp.float32)
    gated = spatial_unit(
        unit_pre, value_pre, spatial_local, bias_local, gain_local, shift_local
    ).astype(jnp.bfloat16)
    token_rows = lax.all_to_all(gated, "tp", split_axis=0, concat_axis=1, tiled=True)
    out_columns = lax.all_gather(w_mix_out, "fs", axis=1, tiled=True)
    out_whole = lax.all_gather(out_columns, "tp", axis=0, tiled=True)
    own_rows = lax.dynamic_slice_in_dim(tokens, row_start, half, 0)
    own_mid = (
        own_rows.astype(jnp.float32)
        + jnp.dot(token_rows, out_whole, preferred_element_type=jnp.float32)
    ).astype(jnp.bfloat16)
    h_mid = lax.all_gather(own_mid, "tp", axis=0, tiled=True)
    normed_mid = rms_scale(h_mid, norm_ffn).astype(jnp.bfloat16)
    gate_whole, up_whole = (
        lax.all_gather(w_gate, "fs", axis=0, tiled=True),
        lax.all_gather(w_up, "fs", axis=0, tiled=True),
    )
    gate = jnp.dot(normed_mid, gate_whole, preferred_element_type=jnp.float32)
    up = jnp.dot(normed_mid, up_whole, preferred_element_type=jnp.float32)
    hidden = (jax.nn.silu(gate) * up).astype(jnp.bfloat16)
    down_cols = lax.all_gather(w_down, "fs", axis=1, tiled=True)
    residual_rows = lax.dynamic_slice_in_dim(h_mid, row_start, half, 0).astype(jnp.float32)
    hidden_rows = lax.all_to_all(hidden, "tp", split_axis=0, concat_axis=1, tiled=True)
    down_full = lax.all_gather(down_cols, "tp", axis=0, tiled=True)
    summed_rows = jnp.dot(hidden_rows, down_full, preferred_element_type=jnp.float32)
    return (residual_rows + summed_rows).astype(jnp.bfloat16)


def solution(mesh):
    placed = (
        P(("rep", "fs"), None),
        P(),
        P("fs", "tp"),
        P("fs", "tp"),
        P(),
        P(),
        P(),
        P(),
        P("tp", "fs"),
        P(),
        P("fs", "tp"),
        P("fs", "tp"),
        P("tp", "fs"),
    )
    return jax.shard_map(
        on_device,
        mesh=mesh,
        in_specs=placed,
        out_specs=P(("rep", "fs", "tp"), None),
        check_vma=False,
    )
```

profile of v0, /device:TPU:0, one launch (start us, length us, event | category | flops | bytes accessed | tf_op | source)
XLA Modules:
  0.0 516.4 jit_solution(7229913326769791295)
XLA Ops:
  6.5 0.7 all-gather.14.cloned.1.call-update
  7.3 0.7 all-gather.12.cloned.1.call-update
  8.8 53.7 %all-gather.14.cloned.1.call-done = bf16[512,2048]{1,0:T(8,128)(2,1)} async-done(((bf16[512,256]{1,0:T(8,128)(2,1)}), bf16[512,2048]{1,0:T(8,128)(2,1)}) %all-gather.14.cloned.1.call-update) | async-done | bytes 2097168 | tf_op jit(solution)/shard_map/all_gather | solution.py:68
  64.5 0.8 dynamic-slice_convert_fusion
  65.3 3.1 fusion
  68.4 43.5 %all-gather.12.cloned.1.call-done = bf16[2048,512]{1,0:T(8,128)(2,1)} async-done(((bf16[256,512]{1,0:T(8,128)(2,1)}), bf16[2048,512]{1,0:T(8,128)(2,1)}) %all-gather.12.cloned.1.call-update) | async-done | bytes 2097168 | tf_op jit(solution)/shard_map/all_gather | solution.py:60
  111.9 6.9 %fusion.21 = f32[1024,512]{1,0:T(8,128)} fusion(bf16[2048,512]{1,0:T(8,128)(2,1)} %all-gather.12.cloned.1.call-done, bf16[1024,2048]{1,0:T(8,128)(2,1)} %param.13, f32[2048]{0:T(1024)S(1)} %convert_element_type.48, f32[1024]{0:T(1024)S(1)} %add_rsqrt_fusion.2), kind=kOutput, calls=%fused_computation.30 | convolution fusion | flops 2160066560 | bytes 8400896 | tf_op jit(solution)/shard_map/dot_general | solution.py:63
  118.8 2.6 reshape.58
  121.4 1.2 reduce_sum.37
  122.6 14.4 %multiply_reduce_fusion = f32[1024,2]{1,0:T(8,128)S(1)} fusion(f32[1024,2,256]{2,1,0:T(2,128)S(1)} %reshape.58, f32[1024,2]{1,0:T(8,128)S(1)} %broadcast_multiply_fusion), kind=kLoop, calls=%fused_computation.33 | loop fusion | flops 1570816 | bytes 2113536 | tf_op jit(solution)/shard_map/reduce_sum | solution.py:19
  137.2 1.2 mul.113
  138.6 1.2 sub.17
  140.4 0.8 add_convert_fusion.2
  142.1 2.3 copy.27
  144.4 1.8 copy.34
  146.2 15.5 %all-gather.10.cloned.1.call-done = bf16[2048,512]{1,0:T(8,128)(2,1)} async-done(((bf16[256,512]{1,0:T(8,128)(2,1)}), bf16[2048,512]{1,0:T(8,128)(2,1)}) %all-gather.10.cloned.1.call-update) | async-done | bytes 2097168 | tf_op jit(solution)/shard_map/all_gather | solution.py:59
  161.7 5.7 %fusion.14 = bf16[1024,512]{1,0:T(8,128)(2,1)S(1)} fusion(f32[1024,512]{1,0:T(8,128)S(1)} %bitcast.40, bf16[2048,512]{1,0:T(8,128)(2,1)} %all-gather.10.cloned.1.call-done, bf16[1024,2048]{1,0:T(8,128)(2,1)} %param.13, f32[2048]{0:T(1024)S(1)} %convert_element_type.48, f32[1024]{0:T(1024)S(1)} %add_rsqrt_fusion.2), kind=kOutput, calls=%fused_computation.23 | convolution fusion | flops 2161115136 | bytes 9449472 | tf_op jit(solution)/shard_map/dot_general | solution.py:62
  168.0 4.6 all_to_all.38
  172.5 2.8 all-gather.16.cloned.1.call-done
  175.3 6.6 %add_convert_fusion.1 = bf16[512,2048]{1,0:T(8,128)(2,1)} fusion(bf16[512,1024]{0,1:T(8,128)(2,1)S(1)} %bitcast.37, bf16[1024,2048]{1,0:T(8,128)(2,1)} %all-gather.16.cloned.1.call-done, bf16[1024,2048]{1,0:T(8,128)(2,1)} %param.13, s32[]{:T(128)S(6)} %select_n.16), kind=kOutput, calls=%fused_computation.12 | convolution fusion | flops 2150629376 | bytes 9437188 | tf_op jit(solution)/shard_map/dot_general | solution.py:73
  182.0 0.7 all-gather.20.cloned.1.call-update
  182.7 0.7 all-gather.22.cloned.1.call-update
  183.5 88.1 %all-gather.24.cloned.1.call-done = bf16[1408,2048]{1,0:T(8,128)(2,1)} async-done(((bf16[1408,256]{1,0:T(8,128)(2,1)}), bf16[1408,2048]{1,0:T(8,128)(2,1)}) %all-gather.24.cloned.1.call-update) | async-done | bytes 5767184 | tf_op jit(solution)/shard_map/all_gather | solution.py:84
  271.6 13.2 %all-gather.18.cloned.1.call-done = bf16[1024,2048]{1,0:T(8,128)(2,1)} async-done(((bf16[512,2048]{1,0:T(8,128)(2,1)}), bf16[1024,2048]{1,0:T(8,128)(2,1)}) %all-gather.18.cloned.1.call-update) | async-done | bytes 4194320 | tf_op jit(solution)/shard_map/all_gather | solution.py:75
  284.8 3.1 fusion.3
  287.9 92.6 %all-gather.20.cloned.1.call-done = bf16[2048,1408]{1,0:T(8,128)(2,1)} async-done(((bf16[256,1408]{1,0:T(8,128)(2,1)}), bf16[2048,1408]{1,0:T(8,128)(2,1)}) %all-gather.20.cloned.1.call-update) | async-done | bytes 5767184 | tf_op jit(solution)/shard_map/all_gather | solution.py:78
  380.5 11.9 %fusion.23 = f32[1024,1408]{1,0:T(8,128)} fusion(bf16[2048,1408]{1,0:T(8,128)(2,1)} %all-gather.20.cloned.1.call-done, bf16[1024,2048]{1,0:T(8,128)(2,1)} %all-gather.18.cloned.1.call-done, f32[2048]{0:T(1024)S(1)} %convert_element_type.57, f32[1024]{0:T(1024)S(1)} %add_rsqrt_fusion.1), kind=kOutput, calls=%fused_computation.34 | convolution fusion | flops 5913968640 | bytes 15740928 | tf_op jit(solution)/shard_map/dot_general | solution.py:81
  392.4 80.8 %all-gather.22.cloned.1.call-done = bf16[2048,1408]{1,0:T(8,128)(2,1)} async-done(((bf16[256,1408]{1,0:T(8,128)(2,1)}), bf16[2048,1408]{1,0:T(8,128)(2,1)}) %all-gather.22.cloned.1.call-update) | async-done | bytes 5767184 | tf_op jit(solution)/shard_map/all_gather | solution.py:79
  473.2 12.5 %multiply_convert_fusion = bf16[1024,1408]{1,0:T(8,128)(2,1)} fusion(f32[1024,1408]{1,0:T(8,128)} %fusion.23, bf16[2048,1408]{1,0:T(8,128)(2,1)} %all-gather.22.cloned.1.call-done, bf16[1024,2048]{1,0:T(8,128)(2,1)} %all-gather.18.cloned.1.call-done, f32[2048]{0:T(1024)S(1)} %convert_element_type.57, f32[1024]{0:T(1024)S(1)} %add_rsqrt_fusion.1), kind=kOutput, calls=%fused_computation.10 | convolution fusion | flops 5922619392 | bytes 18624512 | tf_op jit(solution)/shard_map/dot_general | solution.py:82
  485.7 3.4 copy.29
  489.2 9.1 %all_to_all.39 = bf16[2,512,1408]{1,2,0:T(8,128)(2,1)} all-to-all(bf16[2,512,1408]{1,2,0:T(8,128)(2,1)S(1)} %copy.29), channel_id=1, replica_groups=mesh['rep'=2,'fs'=8,'tp'=2] {'tp'}, dimensions={0} | all-to-all | bytes 5767168 | tf_op jit(solution)/shard_map/all_to_all | solution.py:86
  498.8 11.1 %add_convert_fusion = bf16[512,2048]{1,0:T(8,128)(2,1)} fusion(bf16[512,2816]{0,1:T(8,128)(2,1)} %bitcast.38, bf16[2816,2048]{1,0:T(8,128)(2,1)} %all-gather.26.cloned.1.call-done, bf16[1024,2048]{1,0:T(8,128)(2,1)} %all-gather.18.cloned.1.call-done, s32[]{:T(128)S(6)} %select_n.16), kind=kOutput, calls=%fused_computation.11 | convolution fusion | flops 5908725760 | bytes 18612228 | tf_op jit(solution)/shard_map/dot_general | solution.py:88
  (34 shorter events, 5.7 us)
Async XLA Ops:
  6.5 55.9 %all-gather.14.cloned.1.call-start = ((), (), s32[]{:S(2)}) async-start(), calls=%async_computation.4 | async-start | bytes 2359296 | tf_op jit(solution)/shard_map/all_gather | solution.py:68
  7.3 104.7 %all-gather.12.cloned.1.call-start = ((), (), s32[]{:S(2)}) async-start(), calls=%async_computation.3 | async-start | bytes 2359296 | tf_op jit(solution)/shard_map/all_gather | solution.py:60
  8.0 153.7 %all-gather.10.cloned.1.call-start = ((), (), s32[]{:S(2)}) async-start(), calls=%async_computation.2 | async-start | bytes 2359296 | tf_op jit(solution)/shard_map/all_gather | solution.py:59
  8.7 166.6 %all-gather.16.cloned.1.call-start = ((), (), s32[]{:S(2)}) async-start(), calls=%async_computation.5 | async-start | bytes 6291456 | tf_op jit(solution)/shard_map/all_gather | solution.py:69
  62.5 209.1 %all-gather.24.cloned.1.call-start = ((), (), s32[]{:S(2)}) async-start(), calls=%async_computation.9 | async-start | bytes 6488064 | tf_op jit(solution)/shard_map/all_gather | solution.py:84
  63.1 221.8 %all-gather.18.cloned.1.call-start = ((), (), s32[]{:S(2)}) async-start(), calls=%async_computation.6 | async-start | bytes 6291456 | tf_op jit(solution)/shard_map/all_gather | solution.py:75
  138.6 1.8 copy-start
  140.4 1.1 copy-start.1
  181.9 89.7 %copy-start.2 = (bf16[2048]{0:T(1024)(128)(2,1)S(1)}, bf16[2048]{0:T(1024)(128)(2,1)}, u32[]{:S(2)}) copy-start(bf16[2048]{0:T(1024)(128)(2,1)} %param.22) | copy-start | bytes 12292
  181.9 198.6 %all-gather.20.cloned.1.call-start = ((), (), s32[]{:S(2)}) async-start(), calls=%async_computation.7 | async-start | bytes 6488064 | tf_op jit(solution)/shard_map/all_gather | solution.py:78
  182.7 290.6 %all-gather.22.cloned.1.call-start = ((), (), s32[]{:S(2)}) async-start(), calls=%async_computation.8 | async-start | bytes 6488064 | tf_op jit(solution)/shard_map/all_gather | solution.py:79
  183.4 315.3 %all-gather.26.cloned.1.call-start = ((), (), s32[]{:S(2)}) async-start(), calls=%async_computation.10 | async-start | bytes 17301504 | tf_op jit(solution)/shard_map/all_gather | solution.py:87
Sparse Core Ops, SparseCore 0:
  9.4 53.0 all-gather.13
  64.6 47.2 all-gather.11
  114.0 47.6 all-gather.9
  163.1 12.1 all-gather.15
  177.2 94.2 all-gather.23
  273.0 11.8 all-gather.17
  287.0 93.4 all-gather.19
  382.7 90.4 all-gather.21
  474.8 23.8 all-gather.25
where the time goes:
time: 517 us; the launch traced here: 516 us
  waiting for transfers between devices  395 us (76%)
  matrix products  55.2 us (11%)
  other arithmetic  24.9 us (5%)
  local copies, waits for them, and re-layouts  14.2 us (3%)
  blocking collectives  13.7 us (3%)
  between operations  13.4 us (3%)
    all_gather x1, waiting for transfers between devices, on_device(): lax.all_gather(w_gate, 'fs', axis=0, tiled=True)  92.6 us
    all_gather x1, waiting for transfers between devices, on_device(): down_cols = lax.all_gather(w_down, 'fs', axis=1, tiled=True)  88.1 us
    all_gather x1, waiting for transfers between devices, on_device(): lax.all_gather(w_up, 'fs', axis=0, tiled=True)  80.8 us
    all_gather x1, waiting for transfers between devices, on_device(): out_columns = lax.all_gather(w_mix_out, 'fs', axis=1, tiled=True)  53.7 us
    all_gather x1, waiting for transfers between devices, on_device(): lax.all_gather(w_value, 'fs', axis=0, tiled=True)  43.5 us
    all_gather x1, waiting for transfers between devices, on_device(): lax.all_gather(w_unit, 'fs', axis=0, tiled=True)  15.5 us
    reduce_sum x1, other arithmetic, spatial_unit(): spread = jnp.mean(jnp.square(active - center), axis=-1, keepdims=True)  14.4 us
    all_gather x1, waiting for transfers between devices, on_device(): h_mid = lax.all_gather(own_mid, 'tp', axis=0, tiled=True)  13.2 us
  transfers between devices with their start and end apart: 9, of which 9 were waited for; matrix products, arithmetic and copies ran while one was open for 16% of the time, Pallas kernels for 0%

commit v1 on v0

--- a/solution.py
+++ b/solution.py
@@ -65,7 +65,7 @@
         unit_pre, value_pre, spatial_local, bias_local, gain_local, shift_local
     ).astype(jnp.bfloat16)
     token_rows = lax.all_to_all(gated, "tp", split_axis=0, concat_axis=1, tiled=True)
-    out_columns = lax.all_gather(w_mix_out, "fs", axis=1, tiled=True)
+    out_columns = jnp.concatenate(lax.all_gather(w_mix_out, "fs"), axis=1)
     out_whole = lax.all_gather(out_columns, "tp", axis=0, tiled=True)
     own_rows = lax.dynamic_slice_in_dim(tokens, row_start, half, 0)
     own_mid = (

time: 517 us -> 516 us (level)
  no operation moved by 1% of the time
where the time goes in v1:
time: 516 us
  waiting for transfers between devices  392 us (76%)
  matrix products  55.2 us (11%)
  other arithmetic  22.8 us (4%)
  local copies, waits for them, and re-layouts  18.2 us (4%)
  blocking collectives  13.7 us (3%)
  between operations  13.4 us (3%)
    all_gather x1, waiting for transfers between devices, on_device(): lax.all_gather(w_gate, 'fs', axis=0, tiled=True)  92.6 us
    all_gather x1, waiting for transfers between devices, on_device(): down_cols = lax.all_gather(w_down, 'fs', axis=1, tiled=True)  88.1 us
    all_gather x1, waiting for transfers between devices, on_device(): lax.all_gather(w_up, 'fs', axis=0, tiled=True)  80.8 us
    all_gather x1, waiting for transfers between devices, on_device(): out_columns = jnp.concatenate(lax.all_gather(w_mix_out, 'fs'), axis=1)  52.5 us
    all_gather x1, waiting for transfers between devices, on_device(): lax.all_gather(w_value, 'fs', axis=0, tiled=True)  41.9 us
    all_gather x1, waiting for transfers between devices, on_device(): lax.all_gather(w_unit, 'fs', axis=0, tiled=True)  15.5 us
    reduce_sum x1, other arithmetic, spatial_unit(): spread = jnp.mean(jnp.square(active - center), axis=-1, keepdims=True)  14.4 us
    all_gather x1, waiting for transfers between devices, on_device(): h_mid = lax.all_gather(own_mid, 'tp', axis=0, tiled=True)  13.2 us
  transfers between devices with their start and end apart: 9, of which 9 were waited for; matrix products, arithmetic and copies ran while one was open for 16% of the time, Pallas kernels for 0%

profile of v1, /device:TPU:0, one launch (start us, length us, event | category | flops | bytes accessed | tf_op | source)
XLA Modules:
  0.0 515.6 jit_solution(14128345839930899657)
XLA Ops:
  6.6 0.7 all-gather.27.cloned.1.call-update
  7.3 0.7 all-gather.13.cloned.1.call-update
  8.8 52.5 %all-gather.27.cloned.1.call-done = bf16[4096,256]{1,0:T(8,128)(2,1)} async-done(((bf16[512,256]{1,0:T(8,128)(2,1)}), bf16[4096,256]{1,0:T(8,128)(2,1)}) %all-gather.27.cloned.1.call-update) | async-done | bytes 2097168 | tf_op jit(solution)/shard_map/all_gather | solution.py:68
  61.3 3.9 copy.38
  66.1 3.1 fusion
  69.2 41.9 %all-gather.13.cloned.1.call-done = bf16[2048,512]{1,0:T(8,128)(2,1)} async-done(((bf16[256,512]{1,0:T(8,128)(2,1)}), bf16[2048,512]{1,0:T(8,128)(2,1)}) %all-gather.13.cloned.1.call-update) | async-done | bytes 2097168 | tf_op jit(solution)/shard_map/all_gather | solution.py:60
  111.1 6.9 %fusion.21 = f32[1024,512]{1,0:T(8,128)} fusion(bf16[2048,512]{1,0:T(8,128)(2,1)} %all-gather.13.cloned.1.call-done, bf16[1024,2048]{1,0:T(8,128)(2,1)} %param.13, f32[2048]{0:T(1024)S(1)} %convert_element_type.48, f32[1024]{0:T(1024)S(1)} %add_rsqrt_fusion.2), kind=kOutput, calls=%fused_computation.30 | convolution fusion | flops 2160066560 | bytes 8400896 | tf_op jit(solution)/shard_map/dot_general | solution.py:63
  118.0 2.6 reshape.64
  120.6 1.2 reduce_sum.37
  121.8 14.4 %multiply_reduce_fusion = f32[1024,2]{1,0:T(8,128)S(1)} fusion(f32[1024,2,256]{2,1,0:T(2,128)S(1)} %reshape.64, f32[1024,2]{1,0:T(8,128)S(1)} %broadcast_multiply_fusion), kind=kLoop, calls=%fused_computation.33 | loop fusion | flops 1570816 | bytes 2113536 | tf_op jit(solution)/shard_map/reduce_sum | solution.py:19
  136.3 1.2 mul.113
  137.8 1.2 sub.17
  139.6 0.8 add_convert_fusion.2
  141.3 2.3 copy.36
  143.6 1.8 copy.44
  145.4 15.5 %all-gather.11.cloned.1.call-done = bf16[2048,512]{1,0:T(8,128)(2,1)} async-done(((bf16[256,512]{1,0:T(8,128)(2,1)}), bf16[2048,512]{1,0:T(8,128)(2,1)}) %all-gather.11.cloned.1.call-update) | async-done | bytes 2097168 | tf_op jit(solution)/shard_map/all_gather | solution.py:59
  160.9 5.7 %fusion.14 = bf16[1024,512]{1,0:T(8,128)(2,1)S(1)} fusion(f32[1024,512]{1,0:T(8,128)S(1)} %bitcast.45, bf16[2048,512]{1,0:T(8,128)(2,1)} %all-gather.11.cloned.1.call-done, bf16[1024,2048]{1,0:T(8,128)(2,1)} %param.13, f32[2048]{0:T(1024)S(1)} %convert_element_type.48, f32[1024]{0:T(1024)S(1)} %add_rsqrt_fusion.2), kind=kOutput, calls=%fused_computation.23 | convolution fusion | flops 2161115136 | bytes 9449472 | tf_op jit(solution)/shard_map/dot_general | solution.py:62
  167.1 4.6 all_to_all.38
  171.7 2.8 all-gather.15.cloned.1.call-done
  174.5 6.6 %add_convert_fusion.1 = bf16[512,2048]{1,0:T(8,128)(2,1)} fusion(bf16[512,1024]{0,1:T(8,128)(2,1)S(1)} %bitcast.46, bf16[1024,2048]{0,1:T(8,128)(2,1)} %all-gather.15.cloned.1.call-done, bf16[1024,2048]{1,0:T(8,128)(2,1)} %param.13, s32[]{:T(128)S(6)} %select_n.16), kind=kOutput, calls=%fused_computation.12 | convolution fusion | flops 2150629376 | bytes 9437188 | tf_op jit(solution)/shard_map/dot_general | solution.py:73
  181.2 0.7 all-gather.19.cloned.1.call-update
  181.9 0.7 all-gather.21.cloned.1.call-update
  182.7 88.1 %all-gather.23.cloned.1.call-done = bf16[1408,2048]{1,0:T(8,128)(2,1)} async-done(((bf16[1408,256]{1,0:T(8,128)(2,1)}), bf16[1408,2048]{1,0:T(8,128)(2,1)}) %all-gather.23.cloned.1.call-update) | async-done | bytes 5767184 | tf_op jit(solution)/shard_map/all_gather | solution.py:84
  270.8 13.2 %all-gather.17.cloned.1.call-done = bf16[1024,2048]{1,0:T(8,128)(2,1)} async-done(((bf16[512,2048]{1,0:T(8,128)(2,1)}), bf16[1024,2048]{1,0:T(8,128)(2,1)}) %all-gather.17.cloned.1.call-update) | async-done | bytes 4194320 | tf_op jit(solution)/shard_map/all_gather | solution.py:75
  284.0 3.1 fusion.3
  287.1 92.6 %all-gather.19.cloned.1.call-done = bf16[2048,1408]{1,0:T(8,128)(2,1)} async-done(((bf16[256,1408]{1,0:T(8,128)(2,1)}), bf16[2048,1408]{1,0:T(8,128)(2,1)}) %all-gather.19.cloned.1.call-update) | async-done | bytes 5767184 | tf_op jit(solution)/shard_map/all_gather | solution.py:78
  379.7 11.9 %fusion.23 = f32[1024,1408]{1,0:T(8,128)} fusion(bf16[2048,1408]{1,0:T(8,128)(2,1)} %all-gather.19.cloned.1.call-done, bf16[1024,2048]{1,0:T(8,128)(2,1)} %all-gather.17.cloned.1.call-done, f32[2048]{0:T(1024)S(1)} %convert_element_type.57, f32[1024]{0:T(1024)S(1)} %add_rsqrt_fusion.1), kind=kOutput, calls=%fused_computation.34 | convolution fusion | flops 5913968640 | bytes 15740928 | tf_op jit(solution)/shard_map/dot_general | solution.py:81
  391.6 80.8 %all-gather.21.cloned.1.call-done = bf16[2048,1408]{1,0:T(8,128)(2,1)} async-done(((bf16[256,1408]{1,0:T(8,128)(2,1)}), bf16[2048,1408]{1,0:T(8,128)(2,1)}) %all-gather.21.cloned.1.call-update) | async-done | bytes 5767184 | tf_op jit(solution)/shard_map/all_gather | solution.py:79
  472.4 12.5 %multiply_convert_fusion = bf16[1024,1408]{1,0:T(8,128)(2,1)} fusion(f32[1024,1408]{1,0:T(8,128)} %fusion.23, bf16[2048,1408]{1,0:T(8,128)(2,1)} %all-gather.21.cloned.1.call-done, bf16[1024,2048]{1,0:T(8,128)(2,1)} %all-gather.17.cloned.1.call-done, f32[2048]{0:T(1024)S(1)} %convert_element_type.57, f32[1024]{0:T(1024)S(1)} %add_rsqrt_fusion.1), kind=kOutput, calls=%fused_computation.10 | convolution fusion | flops 5922619392 | bytes 18624512 | tf_op jit(solution)/shard_map/dot_general | solution.py:82
  484.9 3.4 copy.39
  488.4 9.1 %all_to_all.39 = bf16[2,512,1408]{1,2,0:T(8,128)(2,1)} all-to-all(bf16[2,512,1408]{1,2,0:T(8,128)(2,1)S(1)} %copy.39), channel_id=1, replica_groups=mesh['rep'=2,'fs'=8,'tp'=2] {'tp'}, dimensions={0} | all-to-all | bytes 5767168 | tf_op jit(solution)/shard_map/all_to_all | solution.py:86
  497.9 11.1 %add_convert_fusion = bf16[512,2048]{1,0:T(8,128)(2,1)} fusion(bf16[512,2816]{0,1:T(8,128)(2,1)} %bitcast.42, bf16[2816,2048]{1,0:T(8,128)(2,1)} %all-gather.25.cloned.1.call-done, bf16[1024,2048]{1,0:T(8,128)(2,1)} %all-gather.17.cloned.1.call-done, s32[]{:T(128)S(6)} %select_n.16), kind=kOutput, calls=%fused_computation.11 | convolution fusion | flops 5908725760 | bytes 18612228 | tf_op jit(solution)/shard_map/dot_general | solution.py:88
  (43 shorter events, 4.5 us)
Async XLA Ops:
  6.5 59.4 %copy-start.2 = (bf16[2048]{0:T(1024)(128)(2,1)S(1)}, bf16[2048]{0:T(1024)(128)(2,1)}, u32[]{:S(2)}) copy-start(bf16[2048]{0:T(1024)(128)(2,1)} %param.14) | copy-start | bytes 12292
  6.5 59.4 %copy-start.6 = (bf16[4,128]{1,0:T(4,128)(2,1)S(1)}, bf16[4,128]{1,0:T(4,128)(2,1)}, u32[]{:S(2)}) copy-start(bf16[4,128]{1,0:T(4,128)(2,1)} %param.18) | copy-start | bytes 3076
  6.5 59.4 %copy-start.5 = (bf16[1024]{0:T(1024)(128)(2,1)S(1)}, bf16[1024]{0:T(1024)(128)(2,1)}, u32[]{:S(2)}) copy-start(bf16[1024]{0:T(1024)(128)(2,1)} %param.19) | copy-start | bytes 6148
  6.5 59.5 %copy-start.4 = (bf16[1024]{0:T(1024)(128)(2,1)S(1)}, bf16[1024]{0:T(1024)(128)(2,1)}, u32[]{:S(2)}) copy-start(bf16[1024]{0:T(1024)(128)(2,1)} %param.20) | copy-start | bytes 6148
  6.5 54.8 %all-gather.27.cloned.1.call-start = ((), (), s32[]{:S(2)}) async-start(), calls=%async_computation.10 | async-start | bytes 2359296 | tf_op jit(solution)/shard_map/all_gather | solution.py:68
  7.3 103.8 %all-gather.13.cloned.1.call-start = ((), (), s32[]{:S(2)}) async-start(), calls=%async_computation.3 | async-start | bytes 2359296 | tf_op jit(solution)/shard_map/all_gather | solution.py:60
  8.0 152.9 %all-gather.11.cloned.1.call-start = ((), (), s32[]{:S(2)}) async-start(), calls=%async_computation.2 | async-start | bytes 2359296 | tf_op jit(solution)/shard_map/all_gather | solution.py:59
  8.8 165.8 %all-gather.15.cloned.1.call-start = ((), (), s32[]{:S(2)}) async-start(), calls=%async_computation.4 | async-start | bytes 6291456 | tf_op jit(solution)/shard_map/all_gather | solution.py:69
  65.3 205.5 %all-gather.23.cloned.1.call-start = ((), (), s32[]{:S(2)}) async-start(), calls=%async_computation.8 | async-start | bytes 6488064 | tf_op jit(solution)/shard_map/all_gather | solution.py:84
  65.9 218.1 %all-gather.17.cloned.1.call-start = ((), (), s32[]{:S(2)}) async-start(), calls=%async_computation.5 | async-start | bytes 6291456 | tf_op jit(solution)/shard_map/all_gather | solution.py:75
  137.8 1.9 copy-start
  139.6 1.1 copy-start.1
  181.1 89.7 %copy-start.3 = (bf16[2048]{0:T(1024)(128)(2,1)S(1)}, bf16[2048]{0:T(1024)(128)(2,1)}, u32[]{:S(2)}) copy-start(bf16[2048]{0:T(1024)(128)(2,1)} %param.22) | copy-start | bytes 12292
  181.1 198.6 %all-gather.19.cloned.1.call-start = ((), (), s32[]{:S(2)}) async-start(), calls=%async_computation.6 | async-start | bytes 6488064 | tf_op jit(solution)/shard_map/all_gather | solution.py:78
  181.9 290.6 %all-gather.21.cloned.1.call-start = ((), (), s32[]{:S(2)}) async-start(), calls=%async_computation.7 | async-start | bytes 6488064 | tf_op jit(solution)/shard_map/all_gather | solution.py:79
  182.6 315.3 %all-gather.25.cloned.1.call-start = ((), (), s32[]{:S(2)}) async-start(), calls=%async_computation.9 | async-start | bytes 17301504 | tf_op jit(solution)/shard_map/all_gather | solution.py:87
Sparse Core Ops, SparseCore 0:
  9.5 51.7 all-gather.26
  63.4 47.6 all-gather.12
  113.2 47.6 all-gather.10
  162.3 12.1 all-gather.14
  176.4 94.2 all-gather.22
  272.1 11.8 all-gather.16
  286.2 93.4 all-gather.18
  381.9 90.4 all-gather.20
  474.0 23.8 all-gather.24
